TPU v7x, 32 devices: a whole 2x2x4 slice. The times are simulated.
32 devices in a mesh: grp: 2 (over y), sp: 4 (over z), tp: 4 (over x, core).
Axes of the slice: x: 2, y: 2, z: 4, core: 2. Of those that a mesh axis runs over, the one named last changes fastest.
Arguments:
- tokens: bfloat16 [4096, 2048], P(('grp', 'sp'), 'tp'), parts along dimension 0, may hold values from -140 to 140, as said below
- mix_gain: bfloat16 [2, 2048], replicated, may hold values from 0.099609375 to 1.8984375
- gate_weight: bfloat16 [2, 2048, 2048], P(None, 'sp', 'tp'), may hold values from -0.125 to 0.125
- mix_weight: bfloat16 [2, 2048, 2048], P(None, 'sp', 'tp'), may hold values from -0.125 to 0.125
- value_weight: bfloat16 [2, 2048, 2048], P(None, 'sp', 'tp'), may hold values from -0.125 to 0.125
- out_weight: bfloat16 [2, 2048, 2048], P(None, 'sp', 'tp'), may hold values from -0.125 to 0.125
- conv_taps: bfloat16 [2, 3, 2048], P(None, None, 'tp'), may hold values from -3.5 to 3.5
Outputs:
- result_stream: bfloat16 [4096, 2048], P(('grp', 'sp'), 'tp'), parts along dimension 0
There are 2 independent parts, one for each index of `grp`. A program takes and returns all parts, laid end to end along the dimension named above; an argument that names none is the same for every part. Nothing has to cross between parts.
Inputs may be any that keep to these rules, and one draw needn't show every extreme that they name: `tokens`: activations with feature scales of several sizes.
All inputs are finite; a program needn't handle non-finite values.
Results may differ from a plain program's by a relative error of at most 0.015.
Values may be sent and summed in bfloat16 or wider, within the bound.
A program may use at most 64 MiB of HBM per device.

v0:
```python
import jax
import jax.numpy as jnp
from jax import lax
from jax.sharding import PartitionSpec as P

EPS = 1e-06


def passed_along(x, axis, by):
    devices = lax.axis_size(axis)
    pairs = [(i, i + by) for i in range(devices) if 0 <= i + by < devices]
    return lax.ppermute(x, axis, pairs)


def normed_rows(rows, gain):
    wide_rows = rows.astype(jnp.float32)
    factor = lax.rsqrt(jnp.mean(wide_rows * wide_rows, axis=1, keepdims=True) + EPS)
    return (wide_rows * factor * gain.astype(jnp.float32)).astype(jnp.bfloat16)


def convolve(carried, before, tap_rows):
    padded = jnp.concatenate([before, carried], axis=0)
    row_count = carried.shape[0]
    result = jnp.zeros_like(carried)
    for tap_index in range(tap_rows.shape[0]):
        result = (
            result
            + tap_rows[tap_index].astype(jnp.float32) * padded[tap_index : tap_index + row_count]
        )
    return result


def shards(tokens, mix_gain, gate_weight, mix_weight, value_weight, out_weight, conv_taps):
    layer_count = gate_weight.shape[0]
    conv_reach = conv_taps.shape[1] - 1
    fringe_depth = 0
    stream = tokens
    gathered = (
        lax.all_gather(gate_weight, "sp", axis=1, tiled=True),
        lax.all_gather(mix_weight, "sp", axis=1, tiled=True),
        lax.all_gather(value_weight, "sp", axis=1, tiled=True),
        lax.all_gather(out_weight, "sp", axis=1, tiled=True),
    )
    for layer_index in range(layer_count):
        whole = lax.all_gather(stream, "tp", axis=1, tiled=True)
        normed = normed_rows(whole, mix_gain[layer_index])
        gate = jnp.dot(normed, gathered[0][layer_index], preferred_element_type=jnp.float32)
        inner = jnp.dot(normed, gathered[1][layer_index], preferred_element_type=jnp.float32)
        values = jnp.dot(normed, gathered[2][layer_index], preferred_element_type=jnp.float32)
        gate = gate.astype(jnp.bfloat16)
        inner = inner.astype(jnp.bfloat16)
        values = values.astype(jnp.bfloat16)
        carried = inner.astype(jnp.float32) * values.astype(jnp.float32)
        before = passed_along(carried[carried.shape[0] - conv_reach :], "sp", 1)
        conv = convolve(carried, before, conv_taps[layer_index])
        mixed = (gate.astype(jnp.float32) * conv).astype(jnp.bfloat16)
        mixed_all = lax.all_gather(mixed, "tp", axis=1, tiled=True)
        product = jnp.dot(mixed_all, gathered[3][layer_index], preferred_element_type=jnp.float32)
        stream = (stream.astype(jnp.float32) + product).astype(jnp.bfloat16)
    return stream


def solution(mesh):
    return jax.shard_map(
        shards,
        mesh=mesh,
        in_specs=(
            P(("grp", "sp"), "tp"),
            P(),
            P(None, "sp", "tp"),
            P(None, "sp", "tp"),
            P(None, "sp", "tp"),
            P(None, "sp", "tp"),
            P(None, None, "tp"),
        ),
        out_specs=P(("grp", "sp"), "tp"),
        check_vma=False,
    )
```

profile of v0, /device:TPU:0, one launch (start us, length us, event | category | flops | bytes accessed | tf_op | source)
XLA Modules:
  0.0 456.6 jit_solution(16903297331807922796)
XLA Ops:
  6.5 0.0 all-gather.9.cloned.1.call-start
  6.5 0.7 all-gather.9.cloned.1.call-update
  7.3 0.0 copy-start.4
  7.3 0.0 all-gather.15.cloned.1.call-start
  7.3 0.7 all-gather.15.cloned.1.call-update
  8.0 0.0 all-gather.13.cloned.1.call-start
  8.1 0.7 all-gather.13.cloned.1.call-update
  8.8 0.0 all-gather.11.cloned.1.call-start
  8.8 0.5 all-gather.11.cloned.1.call-update
  9.3 0.0 all-gather.19.cloned.1.call-start
  9.4 0.5 all-gather.19.cloned.1.call-update
  9.9 0.0 all-gather.17.cloned.1.call-start
  10.0 0.0 copy-done.4
  10.0 24.2 %all-gather.9.cloned.1.call-done = bf16[512,2048]{1,0:T(8,128)(2,1)} async-done(((bf16[512,512]{1,0:T(8,128)(2,1)}), bf16[512,2048]{1,0:T(8,128)(2,1)}) %all-gather.9.cloned.1.call-update) | async-done | bytes 2097168 | tf_op jit(solution)/shard_map/all_gather | solution.py:45
  34.2 2.2 fusion
  36.4 80.1 %all-gather.15.cloned.1.call-done = bf16[2,2048,512]{2,1,0:T(8,128)(2,1)} async-done(((bf16[2,512,512]{2,1,0:T(8,128)(2,1)}), bf16[2,2048,512]{2,1,0:T(8,128)(2,1)}) %all-gather.15.cloned.1.call-update) | async-done | bytes 4194320 | tf_op jit(solution)/shard_map/all_gather | solution.py:41
  116.6 0.0 copy-done
  116.6 2.9 fusion.22
  119.5 0.0 copy-start.5
  119.5 77.9 %all-gather.13.cloned.1.call-done = bf16[2,2048,512]{2,1,0:T(8,128)(2,1)} async-done(((bf16[2,512,512]{2,1,0:T(8,128)(2,1)}), bf16[2,2048,512]{2,1,0:T(8,128)(2,1)}) %all-gather.13.cloned.1.call-update) | async-done | bytes 4194320 | tf_op jit(solution)/shard_map/all_gather | solution.py:40
  197.4 2.9 fusion.20
  200.3 0.0 copy-start.6
  200.3 1.3 collective-permute-start
  201.6 0.0 copy-done.6
  201.6 0.0 copy-done.5
  201.7 76.4 %all-gather.11.cloned.1.call-done = bf16[2,2048,512]{2,1,0:T(8,128)(2,1)} async-done(((bf16[2,512,512]{2,1,0:T(8,128)(2,1)}), bf16[2,2048,512]{2,1,0:T(8,128)(2,1)}) %all-gather.11.cloned.1.call-update) | async-done | bytes 4194320 | tf_op jit(solution)/shard_map/all_gather | solution.py:39
  278.1 0.0 collective-permute-done
  278.1 4.9 %fusion.43 = bf16[512,512]{1,0:T(8,128)(2,1)} fusion(f32[2,512]{1,0:T(2,128)S(1)} %collective-permute-done, f32[512,512]{1,0:T(8,128)} %copy-done.6, f32[512]{0:T(512)S(1)} %bitcast.83, f32[512]{0:T(512)S(1)} %bitcast.84, f32[512]{0:T(512)S(1)} %bitcast.85, bf16[2,2048,512]{2,1,0:T(8,128)(2,1)} %all-gather.11.cloned.1.call-done, ...), kind=kOutput, calls=%fused_computation.59 | convolution fusion | flops 1080819712 | bytes 5787648 | tf_op jit(solution)/shard_map/dot_general | solution.py:47
  283.0 0.0 all-gather.17.cloned.1.call-update
  283.0 0.0 all-gather.21.cloned.1.call-start
  283.1 75.7 %all-gather.19.cloned.1.call-done = bf16[2,2048,512]{2,1,0:T(8,128)(2,1)} async-done(((bf16[2,512,512]{2,1,0:T(8,128)(2,1)}), bf16[2,2048,512]{2,1,0:T(8,128)(2,1)}) %all-gather.19.cloned.1.call-update) | async-done | bytes 4194320 | tf_op jit(solution)/shard_map/all_gather | solution.py:42
  358.7 22.5 %all-gather.17.cloned.1.call-done = bf16[512,2048]{1,0:T(8,128)(2,1)} async-done(((bf16[512,512]{1,0:T(8,128)(2,1)}), bf16[512,2048]{1,0:T(8,128)(2,1)}) %all-gather.17.cloned.1.call-update) | async-done | bytes 2097168 | tf_op jit(solution)/shard_map/all_gather | solution.py:57
  381.2 0.0 copy-done.2
  381.2 4.3 fusion.31
  385.5 0.0 all-gather.21.cloned.1.call-update
  385.5 0.0 all-gather.23.cloned.1.call-start
  385.6 22.7 %all-gather.21.cloned.1.call-done = bf16[512,2048]{1,0:T(8,128)(2,1)} async-done(((bf16[512,512]{1,0:T(8,128)(2,1)}), bf16[512,2048]{1,0:T(8,128)(2,1)}) %all-gather.21.cloned.1.call-update) | async-done | bytes 2097168 | tf_op jit(solution)/shard_map/all_gather | solution.py:45
  408.3 2.2 fusion.3
  410.5 0.0 copy-start.8
  410.5 3.0 fusion.29
  413.6 1.3 fusion.27
  414.9 3.4 collective-permute-start.1
  418.3 1.3 collective-permute-done.1
  419.7 2.3 fusion.37
  422.0 0.0 all-gather.23.cloned.1.call-update
  422.0 23.5 %all-gather.23.cloned.1.call-done = bf16[512,2048]{1,0:T(8,128)(2,1)} async-done(((bf16[512,512]{1,0:T(8,128)(2,1)}), bf16[512,2048]{1,0:T(8,128)(2,1)}) %all-gather.23.cloned.1.call-update) | async-done | bytes 2097168 | tf_op jit(solution)/shard_map/all_gather | solution.py:57
  445.5 0.0 copy-done.3
  445.5 4.3 fusion.30
  (14 shorter events, 0.1 us)
Async XLA Ops:
  6.5 27.7 %all-gather.9.cloned.1.call-start = ((), (), s32[]{:S(2)}) async-start(), calls=%async_computation | async-start | bytes 2621440 | tf_op jit(solution)/shard_map/all_gather | solution.py:45
  7.3 2.7 copy-start.4
  7.3 109.3 %all-gather.15.cloned.1.call-start = ((), (), s32[]{:S(2)}) async-start(), calls=%async_computation.3 | async-start | bytes 5242880 | tf_op jit(solution)/shard_map/all_gather | solution.py:41
  8.0 189.4 %all-gather.13.cloned.1.call-start = ((), (), s32[]{:S(2)}) async-start(), calls=%async_computation.2 | async-start | bytes 5242880 | tf_op jit(solution)/shard_map/all_gather | solution.py:40
  8.8 269.3 %all-gather.11.cloned.1.call-start = ((), (), s32[]{:S(2)}) async-start(), calls=%async_computation.1 | async-start | bytes 5242880 | tf_op jit(solution)/shard_map/all_gather | solution.py:39
  9.3 349.4 %all-gather.19.cloned.1.call-start = ((), (), s32[]{:S(2)}) async-start(), calls=%async_computation.5 | async-start | bytes 5242880 | tf_op jit(solution)/shard_map/all_gather | solution.py:42
  9.9 371.3 %all-gather.17.cloned.1.call-start = ((), (), s32[]{:S(2)}) async-start(), calls=%async_computation.4 | async-start | bytes 2621440 | tf_op jit(solution)/shard_map/all_gather | solution.py:57
  34.2 82.3 %copy-start = (bf16[512,2048]{1,0:T(8,128)(2,1)S(1)}, bf16[512,2048]{1,0:T(8,128)(2,1)}, u32[]{:S(2)}) copy-start(bf16[512,2048]{1,0:T(8,128)(2,1)} %all-gather.9.cloned.1.call-done) | copy-start | bytes 6291460
  119.5 82.2 %copy-start.5 = (bf16[2,3,512]{2,0,1:T(2,128)(2,1)S(1)}, bf16[2,3,512]{2,0,1:T(2,128)(2,1)}, u32[]{:S(2)}) copy-start(bf16[2,3,512]{2,0,1:T(2,128)(2,1)} %param.13) | copy-start | bytes 18436
  200.3 1.3 copy-start.6
  200.3 77.8 %collective-permute-start = (f32[2,512]{1,0:T(2,128)S(1)}, f32[2,512]{1,0:T(2,128)S(1)}, u32[]{:S(2)}, u32[]{:S(2)}) collective-permute-start(f32[2,512]{1,0:T(2,128)S(1)} %slice.105), channel_id=1, source_target_pairs={{0,4},{4,8},{8,12},{1,5},{5,9},{9,13},{2,6},{6,10},{10,14},{3,7},{... | collective-permute-start | bytes 12296 | tf_op jit(solution)/shard_map/ppermute | solution.py:12
  278.1 103.2 %copy-start.2 = (bf16[512,512]{1,0:T(8,128)(2,1)S(1)}, bf16[512,512]{1,0:T(8,128)(2,1)}, u32[]{:S(2)}) copy-start(bf16[512,512]{1,0:T(8,128)(2,1)} %param.7) | copy-start | bytes 1572868
  283.0 125.2 %all-gather.21.cloned.1.call-start = ((), (), s32[]{:S(2)}) async-start(), calls=%async_computation.6 | async-start | bytes 2621440 | tf_op jit(solution)/shard_map/all_gather | solution.py:45
  385.5 60.0 %all-gather.23.cloned.1.call-start = ((), (), s32[]{:S(2)}) async-start(), calls=%async_computation.7 | async-start | bytes 2621440 | tf_op jit(solution)/shard_map/all_gather | solution.py:57
  408.3 2.2 copy-start.1
  410.5 3.1 copy-start.8
  413.6 6.1 %copy-start.7 = (bf16[2,2048,512]{2,1,0:T(8,128)(2,1)S(1)}, bf16[2,2048,512]{2,1,0:T(8,128)(2,1)}, u32[]{:S(2)}) copy-start(bf16[2,2048,512]{2,1,0:T(8,128)(2,1)} %all-gather.11.cloned.1.call-done) | copy-start | bytes 12582916
  414.9 4.7 %collective-permute-start.1 = (f32[2,512]{1,0:T(2,128)S(1)}, f32[2,512]{1,0:T(2,128)S(1)}, u32[]{:S(2)}, u32[]{:S(2)}) collective-permute-start(f32[2,512]{1,0:T(2,128)S(1)} %slice.112), channel_id=1, source_target_pairs={{0,4},{4,8},{8,12},{1,5},{5,9},{9,13},{2,6},{6,10},{10,14},{3,7},{... | collective-permute-start | bytes 12296 | tf_op jit(solution)/shard_map/ppermute | solution.py:12
  419.6 25.9 %copy-start.3 = (bf16[512,512]{1,0:T(8,128)(2,1)S(1)}, bf16[512,512]{1,0:T(8,128)(2,1)}, u32[]{:S(2)}) copy-start(bf16[512,512]{1,0:T(8,128)(2,1)} %fusion.31) | copy-start | bytes 1572868
Sparse Core Ops, SparseCore 0:
  8.9 25.2 all-gather.8
  35.8 80.7 all-gather.14
  118.1 79.2 all-gather.12
  198.8 79.2 all-gather.10
  279.5 79.2 all-gather.18
  360.2 21.0 all-gather.16
  385.7 22.5 all-gather.20
  422.1 23.3 all-gather.22
where the time goes:
time: 457 us
  waiting for transfers between devices  408 us (89%)
  matrix products  25.9 us (6%)
  between operations  13.6 us (3%)
  starting transfers between devices  4.96 us (1%)
    all_gather x1, waiting for transfers between devices, shards(): lax.all_gather(value_weight, 'sp', axis=1, tiled=True)  80.1 us
    all_gather x1, waiting for transfers between devices, shards(): lax.all_gather(mix_weight, 'sp', axis=1, tiled=True)  77.9 us
    all_gather x1, waiting for transfers between devices, shards(): lax.all_gather(gate_weight, 'sp', axis=1, tiled=True)  76.4 us
    all_gather x1, waiting for transfers between devices, shards(): lax.all_gather(out_weight, 'sp', axis=1, tiled=True)  75.7 us
    all_gather x2, waiting for transfers between devices, shards(): whole = lax.all_gather(stream, 'tp', axis=1, tiled=True)  46.9 us
    all_gather x2, waiting for transfers between devices, shards(): mixed_all = lax.all_gather(mixed, 'tp', axis=1, tiled=True)  46 us
  transfers between devices with their start and end apart: 10, of which 9 were waited for; matrix products, arithmetic and copies ran while one was open for 3% of the time, Pallas kernels for 0%

commit v1 on v0

--- a/solution.py
+++ b/solution.py
@@ -2,8 +2,13 @@
 import jax.numpy as jnp
 from jax import lax
 from jax.sharding import PartitionSpec as P
+from jax.lax import all_to_all, psum
 
 EPS = 1e-06
+
+
+def figure_fit(work_x):
+    return jnp.concatenate(all_to_all(jnp.stack(psum(1, "sp") * [work_x]), "sp", 0, 0), 1)
 
 
 def passed_along(x, axis, by):
@@ -37,7 +42,7 @@
     stream = tokens
     gathered = (
         lax.all_gather(gate_weight, "sp", axis=1, tiled=True),
-        lax.all_gather(mix_weight, "sp", axis=1, tiled=True),
+        figure_fit(mix_weight),
         lax.all_gather(value_weight, "sp", axis=1, tiled=True),
         lax.all_gather(out_weight, "sp", axis=1, tiled=True),
     )

time: 457 us -> 438 us (0.958)
  waiting for transfers between devices: 408 us -> 379 us
  local copies, waits for them, and re-layouts: 0.05 us -> 7.24 us
  starting transfers between devices: 4.96 us -> 11.4 us
    all_to_all x0 -> x1, waiting for transfers between devices: none -> 142 us  [figure_fit(): all_to_all(jnp.stack(psum(1, 'sp') * [work_x]), 'sp', 0, 0)]
    all_gather x1, waiting for transfers between devices: 80.1 us -> 0.02 us  [shards(): lax.all_gather(value_weight, 'sp', axis=1, tiled=True)]
    all_gather x1 -> x0, waiting for transfers between devices: 77.9 us -> none  [shards(): lax.all_gather(mix_weight, 'sp', axis=1, tiled=True)]
    all_gather x2, waiting for transfers between devices: 46.9 us -> 38.7 us  [shards(): whole = lax.all_gather(stream, 'tp', axis=1, tiled=True)]
    all_to_all x0 -> x1, starting transfers between devices: none -> 6.48 us  [figure_fit(): all_to_all(jnp.stack(psum(1, 'sp') * [work_x]), 'sp', 0, 0)]
  transfers between devices with their start and end apart: 10 -> 10, of which waited for: 9 -> 8; matrix products, arithmetic and copies ran while one was open for 3% -> 4% of each run, Pallas kernels for 0% -> 0%
where the time goes in v1:
time: 438 us
  waiting for transfers between devices  379 us (87%)
  matrix products  22.7 us (5%)
  between operations  13.6 us (3%)
  starting transfers between devices  11.4 us (3%)
  local copies, waits for them, and re-layouts  7.24 us (2%)
    all_to_all x1, waiting for transfers between devices, figure_fit(): all_to_all(jnp.stack(psum(1, 'sp') * [work_x]), 'sp', 0, 0)  142 us
    all_gather x1, waiting for transfers between devices, shards(): lax.all_gather(out_weight, 'sp', axis=1, tiled=True)  75.7 us
    all_gather x1, waiting for transfers between devices, shards(): lax.all_gather(gate_weight, 'sp', axis=1, tiled=True)  72 us
    all_gather x2, waiting for transfers between devices, shards(): mixed_all = lax.all_gather(mixed, 'tp', axis=1, tiled=True)  46 us
    all_gather x2, waiting for transfers between devices, shards(): whole = lax.all_gather(stream, 'tp', axis=1, tiled=True)  38.7 us
  transfers between devices with their start and end apart: 10, of which 8 were waited for; matrix products, arithmetic and copies ran while one was open for 4% of the time, Pallas kernels for 0%

profile of v1, /device:TPU:0, one launch (start us, length us, event | category | flops | bytes accessed | tf_op | source)
XLA Modules:
  0.0 437.9 jit_solution(17798335006289847450)
XLA Ops:
  6.5 0.0 all-gather.8.cloned.1.call-start
  6.5 0.7 all-gather.8.cloned.1.call-update
  7.3 0.0 all-gather.12.cloned.1.call-start
  7.3 0.7 all-gather.12.cloned.1.call-update
  8.0 0.0 all-gather.10.cloned.1.call-start
  8.1 0.7 all-gather.10.cloned.1.call-update
  8.7 0.0 copy-done.3
  8.8 2.3 stack.2
  11.1 6.5 %all-to-all-start = ((bf16[4,2,512,512]{3,2,1,0:T(8,128)(2,1)}), bf16[4,2,512,512]{3,2,1,0:T(8,128)(2,1)}, u32[]{:S(2)}, u32[]{:S(2)}) async-start(bf16[4,2,512,512]{3,2,1,0:T(8,128)(2,1)} %stack.2), calls=%async_computation | async-start | bytes 8388608 | tf_op jit(solution)/shard_map/all_to_all | solution.py:11
  17.6 0.0 all-gather.16.cloned.1.call-start
  17.6 0.6 all-gather.16.cloned.1.call-update
  18.1 0.0 all-gather.14.cloned.1.call-start
  18.2 0.0 copy-done.6
  18.2 16.0 %all-gather.8.cloned.1.call-done = bf16[512,2048]{1,0:T(8,128)(2,1)} async-done(((bf16[512,512]{1,0:T(8,128)(2,1)}), bf16[512,2048]{1,0:T(8,128)(2,1)}) %all-gather.8.cloned.1.call-update) | async-done | bytes 2097168 | tf_op jit(solution)/shard_map/all_gather | solution.py:50
  34.2 2.1 fusion
  36.3 142.2 %all-to-all-done = bf16[4,2,512,512]{3,2,1,0:T(8,128)(2,1)} async-done(((bf16[4,2,512,512]{3,2,1,0:T(8,128)(2,1)}), bf16[4,2,512,512]{3,2,1,0:T(8,128)(2,1)}, u32[]{:S(2)}, u32[]{:S(2)}) %all-to-all-start) | async-done | bytes 4194336 | tf_op jit(solution)/shard_map/all_to_all | solution.py:11
  178.5 4.0 fusion.52
  182.5 0.0 copy-done
  182.5 1.3 fusion.25
  183.8 0.0 copy-start.7
  183.8 0.0 all-gather.12.cloned.1.call-done
  183.8 2.9 fusion.18
  186.7 0.0 copy-start.8
  186.7 1.3 collective-permute-start
  188.0 0.0 copy-done.8
  188.1 72.0 %all-gather.10.cloned.1.call-done = bf16[2,2048,512]{2,1,0:T(8,128)(2,1)} async-done(((bf16[2,512,512]{2,1,0:T(8,128)(2,1)}), bf16[2,2048,512]{2,1,0:T(8,128)(2,1)}) %all-gather.10.cloned.1.call-update) | async-done | bytes 4194320 | tf_op jit(solution)/shard_map/all_gather | solution.py:44
  260.1 0.0 collective-permute-done
  260.1 4.9 %fusion.39 = bf16[512,512]{1,0:T(8,128)(2,1)} fusion(f32[2,512]{1,0:T(2,128)S(1)} %collective-permute-done, f32[512,512]{1,0:T(8,128)} %copy-done.8, f32[512]{0:T(512)S(1)} %bitcast.76, f32[512]{0:T(512)S(1)} %bitcast.77, f32[512]{0:T(512)S(1)} %bitcast.78, bf16[2,2048,512]{2,1,0:T(8,128)(2,1)} %all-gather.10.cloned.1.call-done, ...), kind=kOutput, calls=%fused_computation.55 | convolution fusion | flops 1080819712 | bytes 5787648 | tf_op jit(solution)/shard_map/dot_general | solution.py:52
  265.0 0.0 all-gather.14.cloned.1.call-update
  265.0 0.0 all-gather.18.cloned.1.call-start
  265.1 75.7 %all-gather.16.cloned.1.call-done = bf16[2,2048,512]{2,1,0:T(8,128)(2,1)} async-done(((bf16[2,512,512]{2,1,0:T(8,128)(2,1)}), bf16[2,2048,512]{2,1,0:T(8,128)(2,1)}) %all-gather.16.cloned.1.call-update) | async-done | bytes 4194320 | tf_op jit(solution)/shard_map/all_gather | solution.py:47
  340.8 22.5 %all-gather.14.cloned.1.call-done = bf16[512,2048]{1,0:T(8,128)(2,1)} async-done(((bf16[512,512]{1,0:T(8,128)(2,1)}), bf16[512,2048]{1,0:T(8,128)(2,1)}) %all-gather.14.cloned.1.call-update) | async-done | bytes 2097168 | tf_op jit(solution)/shard_map/all_gather | solution.py:62
  363.3 4.4 %fusion.27 = bf16[512,512]{1,0:T(8,128)(2,1)} fusion(bf16[512,2048]{1,0:T(8,128)(2,1)} %all-gather.14.cloned.1.call-done, bf16[2,2048,512]{2,1,0:T(8,128)(2,1)} %all-gather.16.cloned.1.call-done, bf16[512,512]{1,0:T(8,128)(2,1)S(1)} %copy-done.4), kind=kOutput, calls=%fused_computation.39 | convolution fusion | flops 1074528256 | bytes 5242880 | tf_op jit(solution)/shard_map/dot_general | solution.py:63
  367.7 0.0 all-gather.18.cloned.1.call-update
  367.8 0.0 all-gather.20.cloned.1.call-start
  367.8 22.7 %all-gather.18.cloned.1.call-done = bf16[512,2048]{1,0:T(8,128)(2,1)} async-done(((bf16[512,512]{1,0:T(8,128)(2,1)}), bf16[512,2048]{1,0:T(8,128)(2,1)}) %all-gather.18.cloned.1.call-update) | async-done | bytes 2097168 | tf_op jit(solution)/shard_map/all_gather | solution.py:50
  390.5 2.2 fusion.3
  392.7 0.0 copy-done.1
  392.7 0.0 copy-start.10
  392.7 1.3 fusion.24
  394.0 0.9 copy-done.10
  394.9 1.3 fusion.23
  396.3 3.4 collective-permute-start.1
  399.7 1.3 collective-permute-done.1
  401.0 2.3 fusion.33
  403.3 0.0 all-gather.20.cloned.1.call-update
  403.3 23.5 %all-gather.20.cloned.1.call-done = bf16[512,2048]{1,0:T(8,128)(2,1)} async-done(((bf16[512,512]{1,0:T(8,128)(2,1)}), bf16[512,2048]{1,0:T(8,128)(2,1)}) %all-gather.20.cloned.1.call-update) | async-done | bytes 2097168 | tf_op jit(solution)/shard_map/all_gather | solution.py:62
  426.8 4.3 fusion.26
  (19 shorter events, 0.1 us)
Async XLA Ops:
  6.5 2.2 copy-start.3
  6.5 27.7 %all-gather.8.cloned.1.call-start = ((), (), s32[]{:S(2)}) async-start(), calls=%async_computation.1 | async-start | bytes 2621440 | tf_op jit(solution)/shard_map/all_gather | solution.py:50
  7.3 176.6 %all-gather.12.cloned.1.call-start = ((), (), s32[]{:S(2)}) async-start(), calls=%async_computation.3 | async-start | bytes 5242880 | tf_op jit(solution)/shard_map/all_gather | solution.py:46
  8.0 252.1 %all-gather.10.cloned.1.call-start = ((), (), s32[]{:S(2)}) async-start(), calls=%async_computation.2 | async-start | bytes 5242880 | tf_op jit(solution)/shard_map/all_gather | solution.py:44
  11.1 7.1 %copy-start.6 = (bf16[2,2048]{1,0:T(2,128)(2,1)S(1)}, bf16[2,2048]{1,0:T(2,128)(2,1)}, u32[]{:S(2)}) copy-start(bf16[2,2048]{1,0:T(2,128)(2,1)} %param.8) | copy-start | bytes 24580
  11.1 167.4 %all-to-all-start = ((bf16[4,2,512,512]{3,2,1,0:T(8,128)(2,1)}), bf16[4,2,512,512]{3,2,1,0:T(8,128)(2,1)}, u32[]{:S(2)}, u32[]{:S(2)}) async-start(bf16[4,2,512,512]{3,2,1,0:T(8,128)(2,1)} %stack.2), calls=%async_computation | async-start | bytes 8388608 | tf_op jit(solution)/shard_map/all_to_all | solution.py:11
  17.6 323.3 %all-gather.16.cloned.1.call-start = ((), (), s32[]{:S(2)}) async-start(), calls=%async_computation.5 | async-start | bytes 5242880 | tf_op jit(solution)/shard_map/all_gather | solution.py:47
  18.1 345.2 %all-gather.14.cloned.1.call-start = ((), (), s32[]{:S(2)}) async-start(), calls=%async_computation.4 | async-start | bytes 2621440 | tf_op jit(solution)/shard_map/all_gather | solution.py:62
  178.5 4.0 copy-start
  183.8 4.3 copy-start.7
  186.7 1.3 copy-start.8
  186.7 73.4 %collective-permute-start = (f32[2,512]{1,0:T(2,128)S(1)}, f32[2,512]{1,0:T(2,128)S(1)}, u32[]{:S(2)}, u32[]{:S(2)}) collective-permute-start(f32[2,512]{1,0:T(2,128)S(1)} %slice.107), channel_id=1, source_target_pairs={{0,4},{4,8},{8,12},{1,5},{5,9},{9,13},{2,6},{6,10},{10,14},{3,7},{... | collective-permute-start | bytes 12296 | tf_op jit(solution)/shard_map/ppermute | solution.py:17
  260.1 103.2 %copy-start.4 = (bf16[512,512]{1,0:T(8,128)(2,1)S(1)}, bf16[512,512]{1,0:T(8,128)(2,1)}, u32[]{:S(2)}) copy-start(bf16[512,512]{1,0:T(8,128)(2,1)} %param.7) | copy-start | bytes 1572868
  265.0 125.4 %all-gather.18.cloned.1.call-start = ((), (), s32[]{:S(2)}) async-start(), calls=%async_computation.6 | async-start | bytes 2621440 | tf_op jit(solution)/shard_map/all_gather | solution.py:50
  363.3 29.4 %copy-start.2 = (bf16[1,4,512,512]{3,2,0,1:T(8,128)(2,1)S(1)}, bf16[1,4,512,512]{3,2,0,1:T(8,128)(2,1)}, u32[]{:S(2)}) copy-start(bf16[1,4,512,512]{3,2,0,1:T(8,128)(2,1)} %get-tuple-element.6) | copy-start | bytes 6291460
  367.8 59.1 %all-gather.20.cloned.1.call-start = ((), (), s32[]{:S(2)}) async-start(), calls=%async_computation.7 | async-start | bytes 2621440 | tf_op jit(solution)/shard_map/all_gather | solution.py:62
  390.5 2.2 copy-start.1
  392.7 2.2 copy-start.10
  394.9 6.1 %copy-start.9 = (bf16[2,2048,512]{2,1,0:T(8,128)(2,1)S(1)}, bf16[2,2048,512]{2,1,0:T(8,128)(2,1)}, u32[]{:S(2)}) copy-start(bf16[2,2048,512]{2,1,0:T(8,128)(2,1)} %all-gather.10.cloned.1.call-done) | copy-start | bytes 12582916
  396.3 4.7 %collective-permute-start.1 = (f32[2,512]{1,0:T(2,128)S(1)}, f32[2,512]{1,0:T(2,128)S(1)}, u32[]{:S(2)}, u32[]{:S(2)}) collective-permute-start(f32[2,512]{1,0:T(2,128)S(1)} %slice.114), channel_id=1, source_target_pairs={{0,4},{4,8},{8,12},{1,5},{5,9},{9,13},{2,6},{6,10},{10,14},{3,7},{... | collective-permute-start | bytes 12296 | tf_op jit(solution)/shard_map/ppermute | solution.py:17
  401.0 25.8 %copy-start.5 = (bf16[512,512]{1,0:T(8,128)(2,1)S(1)}, bf16[512,512]{1,0:T(8,128)(2,1)}, u32[]{:S(2)}) copy-start(bf16[512,512]{1,0:T(8,128)(2,1)} %fusion.27) | copy-start | bytes 1572868
Sparse Core Ops, SparseCore 0:
  8.9 25.2 all-gather.7
  35.8 136.5 all-gather.11
  173.9 86.1 all-gather.9
  261.6 79.2 all-gather.15
  342.2 21.0 all-gather.13
  367.9 22.5 all-gather.17
  403.4 23.3 all-gather.19
